TPU v7x, 32 devices: a whole 2x2x4 slice. The times are simulated.
32 devices in a mesh: sp: 8 (over z, x), tp: 4 (over y, core).
Axes of the slice: x: 2, y: 2, z: 4, core: 2. Of those that a mesh axis runs over, the one named last changes fastest.
Arguments:
- pool_input: bfloat16 [2048, 256], P('sp', 'tp'), may hold values from -6 to 6
- pool_weight: bfloat16 [4, 64, 64], P('tp'), may hold values from -0.75 to 0.75
- pool_gain: bfloat16 [256], P('tp'), may hold values from 0.099609375 to 1.8984375
- out_weight: bfloat16 [256, 2048], P(None, 'tp'), may hold values from -0.375 to 0.375
- resid: bfloat16 [2048, 2048], P('sp', 'tp'), may hold values from -90 to 90
- norm_gain: bfloat16 [2048], P('tp'), may hold values from 0.099609375 to 1.8984375
- routes: int32 [2048, 2], P('sp'), may hold values from 0 to 7, all different within a row; in each aligned block of 256 rows (0 to 255, 256 to 511, ...) at most 128 rows name the same one
- route_weight: float32 [2048, 2], P('sp'), may hold values from 0.2 to 1
- expert_gate: bfloat16 [8, 2048, 4096], P('sp', None, 'tp'), may hold values from -0.375 to 0.375
- expert_up: bfloat16 [8, 2048, 4096], P('sp', None, 'tp'), may hold values from -0.375 to 0.375
- expert_down: bfloat16 [8, 4096, 2048], P('sp', 'tp'), may hold values from -0.0234375 to 0.0234375
Outputs:
- layer_out: bfloat16 [2048, 2048], P('sp', 'tp')
Inputs may be any that keep to these rules, and one draw needn't show every extreme that they name: `routes`: the 2 experts of a position differ. In each aligned block of 256 positions no expert is named by more than 128 assignments; some block reaches that bound.
All inputs are finite; a program needn't handle non-finite values.
Results may differ from a plain program's by a relative error of at most 0.0085.
Values may be sent and summed in bfloat16 or wider, within the bound.
A program may use at most 64 MiB of HBM per device.

v0:
```python
import jax
import jax.numpy as jnp
from jax import lax
from jax.sharding import PartitionSpec as P

D = 2048
GSIZE = 64
REACH = 16
TOPK = 2


GATE_LIMIT = 7.0
GATE_ALPHA = 1.702
NORM_EPS = 1e-05


def from_behind(value, axis, steps):
    count = lax.axis_size(axis)
    first, last = (max(0, -steps), min(count, count - steps))
    return lax.ppermute(value, axis, [(source, source + steps) for source in range(first, last)])


def clamped_unit(gate_pre, up_pre):
    gate_cut = jnp.minimum(gate_pre, GATE_LIMIT)
    up_cut = jnp.clip(up_pre, -GATE_LIMIT, GATE_LIMIT)
    return (up_cut + 1.0) * gate_cut * jax.nn.sigmoid(GATE_ALPHA * gate_cut)


def window_pool(extended, width_of, position, tok_count):
    summed = jnp.zeros((tok_count, extended.shape[1]), jnp.float32)
    for offset in range(REACH):
        first_row = REACH - 1 - offset
        shifted = extended[first_row : first_row + tok_count]
        summed = summed + jnp.where(offset < width_of[None, :], shifted, 0.0)
    counted = jnp.minimum(position[:, None] + 1, width_of[None, :]).astype(jnp.float32)
    current = extended[REACH - 1 :]
    return (summed / counted - current).astype(jnp.bfloat16)


def slot_of(route_block, expert_count, capacity):
    flattened = route_block.reshape(-1)
    onehot = (flattened[:, None] == jnp.arange(expert_count, dtype=jnp.int32)[None, :]).astype(
        jnp.int32
    )
    earlier = jnp.cumsum(onehot, axis=0) - onehot
    ranked = jnp.sum(earlier * onehot, axis=1)
    return flattened * capacity + ranked


def on_device(
    pool_input,
    pool_weight,
    pool_gain,
    out_weight,
    resid,
    norm_gain,
    routes,
    route_weight,
    expert_gate,
    expert_up,
    expert_down,
):
    tok_rows, channels = pool_input.shape
    groups = pool_weight.shape[0]
    features = out_weight.shape[1]
    experts_all = lax.axis_size("sp") * expert_gate.shape[0]
    capacity = 2 * tok_rows * TOPK // experts_all
    tail_rows = pool_input[tok_rows - (REACH - 1) :]
    before = from_behind(tail_rows, "sp", 1)
    extended = jnp.concatenate([before, pool_input], axis=0).astype(jnp.float32)
    first_group = lax.axis_index("tp") * groups
    width_of = 2 ** (1 + (first_group + jnp.arange(channels, dtype=jnp.int32) // GSIZE) % 4)
    position = lax.axis_index("sp") * tok_rows + jnp.arange(tok_rows, dtype=jnp.int32)
    pooled = window_pool(extended, width_of, position, tok_rows)
    grouped = jnp.einsum(
        "tgc,gcd->tgd",
        pooled.reshape(tok_rows, groups, GSIZE),
        pool_weight,
        preferred_element_type=jnp.float32,
    )
    mixed_out = (
        (grouped * pool_gain.astype(jnp.float32).reshape(groups, GSIZE))
        .astype(jnp.bfloat16)
        .reshape(tok_rows, channels)
    )
    projected = jnp.dot(
        lax.all_gather(mixed_out, "tp", axis=1, tiled=True),
        out_weight,
        preferred_element_type=jnp.float32,
    )
    stored = lax.optimization_barrier((resid.astype(jnp.float32) + projected).astype(jnp.bfloat16))
    stream = stored.astype(jnp.float32)
    squares = lax.psum(jnp.sum(stream * stream, axis=1), "tp")
    scale_row = lax.rsqrt(squares / D + NORM_EPS)
    normed_part = (stream * scale_row[:, None] * norm_gain.astype(jnp.float32)).astype(jnp.bfloat16)
    slot_index = slot_of(routes, experts_all, capacity)
    token_ids = jnp.repeat(jnp.arange(tok_rows, dtype=jnp.int32), TOPK)
    slot_token = (
        jnp.full((experts_all * capacity,), tok_rows, jnp.int32).at[slot_index].set(token_ids)
    )
    sent_rows = jnp.take(normed_part, slot_token, axis=0, mode="fill", fill_value=0).reshape(
        experts_all, capacity, features
    )
    gathered = lax.all_gather(
        lax.all_to_all(sent_rows, "sp", split_axis=0, concat_axis=0, tiled=True),
        "tp",
        axis=2,
        tiled=True,
    )
    sources = gathered.shape[0]
    slot_count = gathered.shape[1]
    flattened = gathered.reshape(sources * slot_count, gathered.shape[2])
    gate_pre = jnp.dot(flattened, expert_gate[0], preferred_element_type=jnp.float32)
    up_pre = jnp.dot(flattened, expert_up[0], preferred_element_type=jnp.float32)
    hidden = clamped_unit(gate_pre, up_pre).astype(jnp.bfloat16)
    down_piece = expert_down[0]
    summed = lax.psum_scatter(
        lax.dot_general(
            down_piece, hidden, (((0,), (1,)), ((), ())), preferred_element_type=jnp.float32
        ).astype(jnp.bfloat16),
        "tp",
        scatter_dimension=0,
        tiled=True,
    ).astype(jnp.float32)
    result = summed.astype(jnp.bfloat16).reshape(summed.shape[0], sources, slot_count)
    returned = lax.all_to_all(result, "sp", split_axis=1, concat_axis=1, tiled=True)
    flat_back = returned.reshape(returned.shape[0], experts_all * capacity)
    picked = (
        jnp.take(flat_back, slot_index, axis=1)
        .astype(jnp.float32)
        .reshape(flat_back.shape[0], tok_rows, TOPK)
    )
    combined = jnp.sum(picked * route_weight[None, :, :], axis=2)
    return (stream + combined.T).astype(jnp.bfloat16)


def solution(mesh):
    in_specs = (
        P("sp", "tp"),
        P("tp", None, None),
        P("tp"),
        P(None, "tp"),
        P("sp", "tp"),
        P("tp"),
        P("sp", None),
        P("sp", None),
        P("sp", None, "tp"),
        P("sp", None, "tp"),
        P("sp", "tp", None),
    )
    out_specs = P("sp", "tp")
    return jax.shard_map(
        on_device, mesh=mesh, in_specs=in_specs, out_specs=out_specs, check_vma=False
    )
```

profile of v0, /device:TPU:0, one launch (start us, length us, event | category | flops | bytes accessed | tf_op | source)
XLA Modules:
  0.0 210.5 jit_solution(373483035602310403)
XLA Ops:
  6.5 0.8 slice.58
  7.4 4.9 %collective-permute-start = (bf16[15,64]{0,1:T(8,128)(2,1)S(1)}, bf16[15,64]{0,1:T(8,128)(2,1)S(1)}, u32[]{:S(2)}, u32[]{:S(2)}) collective-permute-start(bf16[15,64]{0,1:T(8,128)(2,1)S(1)} %slice.58), channel_id=1, source_target_pairs={{0,4},{4,8},{8,12},{12,16},{16,20},{20,24},{24,28},{1,5},{5,9},{9,... | collective-permute-start | bytes 5768 | tf_op jit(solution)/shard_map/ppermute | solution.py:20
  12.5 0.8 copy.18
  13.3 0.1 eq.28
  13.4 0.1 reshape.227
  13.6 0.7 broadcast_multiply_fusion
  14.3 1.1 reduce-window.6
  15.4 0.2 slice_reduce_fusion
  15.8 0.1 mul.320
  16.2 2.4 %scatter_custom_fusion = s32[1024]{0:T(1024)S(1)} fusion(s32[512]{0:T(512)S(1)} %bitcast.63, s32[512]{0:T(512)S(1)} %reshape.253, s32[]{:T(128)} %constant.149.clone.1), kind=kCustom, calls=%fused_computation.79 | custom fusion | bytes 4100 | tf_op jit(solution)/shard_map/scatter | solution.py:99
  18.7 0.7 convert_element_type.62
  19.4 0.7 convert_element_type.69
  20.1 0.8 maximum_convert_fusion
  20.9 1.3 fusion.13
  22.2 5.4 %all-gather = bf16[256,1,256]{0,2,1:T(8,128)(2,1)S(1)} all-gather(bf16[256,1,64]{0,2,1:T(8,128)(2,1)S(1)} %fusion.13), channel_id=2, replica_groups=mesh['sp'=8,'tp'=4] {'tp'}, dimensions={2}, use_global_device_ids=true | all-gather | bytes 163840 | tf_op jit(solution)/shard_map/all_gather | solution.py:87
  27.7 1.2 fusion.10
  29.0 7.1 %psum.7 = f32[256]{0:T(256)S(1)} all-reduce(f32[256]{0:T(256)S(1)} %fusion.14), channel_id=1, replica_groups=mesh['sp'=8,'tp'=4] {'tp'}, use_global_device_ids=true, to_apply=%region_5.6 | all-reduce | flops 256 | bytes 2048 | tf_op jit(solution)/shard_map/psum | solution.py:93
  36.3 4.0 %gather_fusion = bf16[1024,512]{1,0:T(8,128)(2,1)S(1)} fusion(bf16[256,512]{1,0:T(8,128)(2,1)S(1)} %fusion.16, s32[1024]{0:T(1024)S(1)} %fusion.42), kind=kCustom, calls=%fused_computation | custom fusion | bytes 2101248 | tf_op jit(solution)/shard_map/jit(_take)/gather | solution.py:101
  40.2 0.2 broadcast_select_fusion
  40.5 29.1 %all_to_all.10 = bf16[8,128,512]{2,1,0:T(8,128)(2,1)} all-to-all(bf16[8,128,512]{2,1,0:T(8,128)(2,1)S(1)} %broadcast_select_fusion), channel_id=1, replica_groups=mesh['sp'=8,'tp'=4] {'sp'}, dimensions={0} | all-to-all | bytes 2097152 | tf_op jit(solution)/shard_map/all_to_all | solution.py:105
  69.7 33.6 %all-gather.3.cloned.1.call-done = bf16[8,128,2048]{2,1,0:T(8,128)(2,1)} async-done(((bf16[8,128,512]{2,1,0:T(8,128)(2,1)}), bf16[8,128,2048]{2,1,0:T(8,128)(2,1)}) %all-gather.3.cloned.1.call-update) | async-done | bytes 4194320 | tf_op jit(solution)/shard_map/all_gather | solution.py:104
  103.3 7.6 %fusion.2 = f32[1024,1024]{1,0:T(8,128)S(1)} fusion(bf16[1024,2048]{1,0:T(8,128)(2,1)} %bitcast.65, bf16[1,2048,1024]{2,1,0:T(8,128)(2,1)} %param.19), kind=kOutput, calls=%fused_computation.5 | convolution fusion | flops 4294967296 | bytes 12582912 | tf_op jit(solution)/shard_map/dot_general | solution.py:113
  110.9 5.7 %multiply_convert_fusion = bf16[1024,1024]{1,0:T(8,128)(2,1)S(1)} fusion(f32[1024,1024]{1,0:T(8,128)S(1)} %fusion.2, bf16[1024,2048]{1,0:T(8,128)(2,1)S(1)} %bitcast.66, bf16[1,2048,1024]{2,1,0:T(8,128)(2,1)S(1)} %copy-done.3), kind=kOutput, calls=%fused_computation.10 | convolution fusion | flops 4305453056 | bytes 14680064 | tf_op jit(solution)/shard_map/dot_general | solution.py:114
  116.6 6.1 %convert_bitcast_fusion = bf16[2048,1024]{0,1:T(8,128)(2,1)} fusion(bf16[1024,1024]{1,0:T(8,128)(2,1)S(1)} %multiply_convert_fusion, bf16[1,1024,2048]{2,1,0:T(8,128)(2,1)S(1)} %copy-done.4), kind=kOutput, calls=%fused_computation.9 | convolution fusion | flops 4297064448 | bytes 10485760 | tf_op jit(solution)/shard_map/dot_general | solution.py:118
  122.7 44.6 %reduce-scatter.2.cloned.1.call-done = bf16[512,1024]{0,1:T(8,128)(2,1)} async-done(((bf16[2048,1024]{0,1:T(8,128)(2,1)}), bf16[512,1024]{0,1:T(8,128)(2,1)}) %reduce-scatter.2.cloned.1.call-update) | async-done | bytes 1048592 | tf_op jit(solution)/shard_map/reduce_scatter | solution.py:117
  167.3 5.5 %all-to-all-start.1 = ((bf16[512,8,128]{0,2,1:T(8,128)(2,1)}), bf16[512,8,128]{0,2,1:T(8,128)(2,1)S(1)}, u32[]{:S(2)}, u32[]{:S(2)}) async-start(bf16[512,8,128]{0,2,1:T(8,128)(2,1)} %bitcast.61), calls=%async_computation.2 | async-start | bytes 2097152 | tf_op jit(solution)/shard_map/all_to_all | solution.py:126
  173.0 0.2 copy.21
  173.4 25.1 %all-to-all-done.1 = bf16[512,8,128]{0,2,1:T(8,128)(2,1)S(1)} async-done(((bf16[512,8,128]{0,2,1:T(8,128)(2,1)}), bf16[512,8,128]{0,2,1:T(8,128)(2,1)S(1)}, u32[]{:S(2)}, u32[]{:S(2)}) %all-to-all-start.1) | async-done | bytes 1048608 | tf_op jit(solution)/shard_map/all_to_all | solution.py:126
  198.5 2.0 gather_fusion.1
  200.4 0.2 gather.15
  200.6 2.2 %multiply_reduce_fusion = f32[512,256]{0,1:T(8,128)S(1)} fusion(bf16[512,256,2]{0,2,1:T(2,128)(2,1)S(1)} %gather.15, pred[256,2]{1,0:T(8,128)(4,1)S(1)} %copy.21, f32[256,2]{1,0:T(8,128)S(1)} %copy.23), kind=kLoop, calls=%fused_computation.17 | loop fusion | flops 917504 | bytes 1051136 | tf_op jit(solution)/shard_map/reduce_sum | solution.py:133
  202.9 0.8 fusion.17
  (45 shorter events, 1.4 us)
Async XLA Ops:
  6.5 21.1 %copy-start = (bf16[256,512]{1,0:T(8,128)(2,1)S(1)}, bf16[256,512]{1,0:T(8,128)(2,1)}, u32[]{:S(2)}) copy-start(bf16[256,512]{1,0:T(8,128)(2,1)} %param.14) | copy-start | bytes 786436
  6.5 96.7 %all-gather.3.cloned.1.call-start = ((), (), s32[]{:S(2)}) async-start(), calls=%async_computation.3 | async-start | bytes 5242880 | tf_op jit(solution)/shard_map/all_gather | solution.py:104
  7.4 12.7 %collective-permute-start = (bf16[15,64]{0,1:T(8,128)(2,1)S(1)}, bf16[15,64]{0,1:T(8,128)(2,1)S(1)}, u32[]{:S(2)}, u32[]{:S(2)}) collective-permute-start(bf16[15,64]{0,1:T(8,128)(2,1)S(1)} %slice.58), channel_id=1, source_target_pairs={{0,4},{4,8},{8,12},{12,16},{16,20},{20,24},{24,28},{1,5},{5,9},{9,... | collective-permute-start | bytes 5768 | tf_op jit(solution)/shard_map/ppermute | solution.py:20
  69.6 97.7 %reduce-scatter.2.cloned.1.call-start = ((), (), s32[]{:S(2)}) async-start(), calls=%async_computation.4 | async-start | bytes 5242880 | tf_op jit(solution)/shard_map/reduce_scatter | solution.py:117
  103.3 7.7 %copy-start.3 = (bf16[1,2048,1024]{2,1,0:T(8,128)(2,1)S(1)}, bf16[1,2048,1024]{2,1,0:T(8,128)(2,1)}, u32[]{:S(2)}) copy-start(bf16[1,2048,1024]{2,1,0:T(8,128)(2,1)} %param.20) | copy-start | bytes 12582916
  103.3 7.7 %copy-start.5 = (bf16[8,128,2048]{2,1,0:T(8,128)(2,1)S(1)}, bf16[8,128,2048]{2,1,0:T(8,128)(2,1)}, u32[]{:S(2)}) copy-start(bf16[8,128,2048]{2,1,0:T(8,128)(2,1)} %all-gather.3.cloned.1.call-done) | copy-start | bytes 12582916
  110.9 5.7 %copy-start.4 = (bf16[1,1024,2048]{2,1,0:T(8,128)(2,1)S(1)}, bf16[1,1024,2048]{2,1,0:T(8,128)(2,1)}, u32[]{:S(2)}) copy-start(bf16[1,1024,2048]{2,1,0:T(8,128)(2,1)} %param.21) | copy-start | bytes 12582916
  122.7 50.3 %copy-start.1 = (s32[256,2]{0,1:T(2,128)S(1)}, s32[256,2]{0,1:T(2,128)}, u32[]{:S(2)}) copy-start(s32[256,2]{0,1:T(2,128)} %param.17) | copy-start | bytes 6148
  122.7 50.5 %copy-start.2 = (f32[256,2]{0,1:T(2,128)S(1)}, f32[256,2]{0,1:T(2,128)}, u32[]{:S(2)}) copy-start(f32[256,2]{0,1:T(2,128)} %param.18) | copy-start | bytes 6148
  167.3 31.2 %all-to-all-start.1 = ((bf16[512,8,128]{0,2,1:T(8,128)(2,1)}), bf16[512,8,128]{0,2,1:T(8,128)(2,1)S(1)}, u32[]{:S(2)}, u32[]{:S(2)}) async-start(bf16[512,8,128]{0,2,1:T(8,128)(2,1)} %bitcast.61), calls=%async_computation.2 | async-start | bytes 2097152 | tf_op jit(solution)/shard_map/all_to_all | solution.py:126
Sparse Core Ops, SparseCore 0:
  69.7 33.4 all-gather.2
  122.8 44.3 reduce-scatter.1
where the time goes:
time: 211 us; the launch traced here: 210 us
  waiting for transfers between devices  103 us (49%)
  blocking collectives  41.7 us (20%)
  matrix products  21.9 us (10%)
  between operations  13.7 us (6%)
  local copies, waits for them, and re-layouts  11.7 us (6%)
  starting transfers between devices  10.4 us (5%)
  other arithmetic  7.86 us (4%)
    reduce_scatter x1, waiting for transfers between devices, on_device(): lax.psum_scatter(lax.dot_general(down_piece, hidden, (((0,), (1,)), ((),...  44.6 us
    all_gather x1, waiting for transfers between devices, on_device(): lax.all_gather(lax.all_to_all(sent_rows, 'sp', split_axis=0, concat_axis=...  33.6 us
    all_to_all x1, blocking collectives, on_device(): lax.all_to_all(sent_rows, 'sp', split_axis=0, concat_axis=0, tiled=True)  29.1 us
    all_to_all x1, waiting for transfers between devices, on_device(): lax.all_to_all(result, 'sp', split_axis=1, concat_axis=1, tiled=True)  25.1 us
    dot_general x1, matrix products, on_device(): jnp.dot(flattened, expert_gate[0], preferred_element_type=jnp.float32)  7.64 us
    psum x1, blocking collectives, on_device(): squares = lax.psum(jnp.sum(stream * stream, axis=1), 'tp')  7.13 us
    dot_general x1, matrix products, on_device(): lax.dot_general(down_piece, hidden, (((0,), (1,)), ((), ())), preferred_e...  6.07 us
    dot_general x1, matrix products, on_device(): jnp.dot(flattened, expert_up[0], preferred_element_type=jnp.float32)  5.66 us
  transfers between devices with their start and end apart: 4, of which 3 were waited for; matrix products, arithmetic and copies ran while one was open for 4% of the time, Pallas kernels for 0%

commit v1 on v0

v1 whole, which is shorter than its diff:
```python
import functools

import jax
import jax.numpy as jnp
from jax import lax
from jax.experimental import pallas as pl
from jax.experimental.pallas import tpu as pltpu
from jax.sharding import PartitionSpec as P

GSIZE = 64
REACH = 16
TOPK = 2
CORES = 2
LANES = 128
CHUNK_ROWS = 256

GATE_LIMIT = 7.0
GATE_ALPHA = 1.702
NORM_EPS = 1e-05

F32 = jnp.float32
BF16 = jnp.bfloat16
MESH = pl.DeviceIdType.MESH


def from_behind(value, axis, steps):
    count = lax.axis_size(axis)
    first, last = (max(0, -steps), min(count, count - steps))
    return lax.ppermute(value, axis, [(source, source + steps) for source in range(first, last)])


def window_pool(extended, width_of, position, tok_count):
    summed = jnp.zeros((tok_count, extended.shape[1]), F32)
    for offset in range(REACH):
        first_row = REACH - 1 - offset
        shifted = extended[first_row : first_row + tok_count]
        summed = summed + jnp.where(offset < width_of[None, :], shifted, 0.0)
    counted = jnp.minimum(position[:, None] + 1, width_of[None, :]).astype(F32)
    current = extended[REACH - 1 :]
    return (summed / counted - current).astype(BF16)


def dot(a, b):
    return jnp.dot(a, b, preferred_element_type=F32)


def moe_kernel(
    n, tp, cap,
    stream_ref, normed_ref, routes_ref, weight_ref, gate_hbm, up_hbm, down_hbm,
    out_ref,
    x, sent, wg, wu, wd, hidden, own, mine, pc_send, pc_recv, ys_send, ys_recv, res, ret, acc,
    w_sem, a_send, a_recv, b_send, b_recv, c_send, c_recv, d_send, d_recv, e_send, e_recv, f_send, f_recv,
):
    ny = tp // CORES
    tok, feat = normed_ref.shape
    width = wg.shape[1]
    group = x.shape[0] // ys_send.shape[0]
    chunks = n // group
    rows = group * cap
    sp = lax.axis_index("sp")
    t = lax.axis_index("tp")
    y, core = t // CORES, t % CORES
    partner = y * CORES + (1 - core)

    loads = [
        pltpu.make_async_copy(gate_hbm.at[0], wg, w_sem.at[0]),
        pltpu.make_async_copy(up_hbm.at[0], wu, w_sem.at[1]),
        pltpu.make_async_copy(down_hbm.at[0], wd, w_sem.at[2]),
    ]
    for load in loads:
        load.start()

    barrier = pltpu.get_barrier_semaphore()
    peers = [(lax.rem(sp + d, n), t) for d in range(1, n)]
    peers += [(sp, lax.rem(y + k, ny) * CORES + core) for k in range(1, ny)]
    peers += [(sp, partner)]
    for peer in peers:
        pl.semaphore_signal(barrier, inc=1, device_id=peer, device_id_type=MESH)

    def cols(block):
        return pl.ds(pl.multiple_of(block * feat, LANES), feat)

    def remote(src, dst, send, recv, device):
        return pltpu.make_async_remote_copy(
            src_ref=src, dst_ref=dst, send_sem=send, recv_sem=recv, device_id=device, device_id_type=MESH
        )

    def copy_a(d):
        return remote(sent.at[d], x.at[d, :, cols(t)], a_send.at[d], a_recv.at[d], (lax.rem(sp + d, n), t))

    def copy_b(d, k):
        part = x.at[d, :, cols(t)]
        return remote(part, part, b_send.at[d, k], b_recv.at[d, k], (sp, lax.rem(y + k, ny) * CORES + core))

    def copy_c(d, k):
        part = x.at[d, :, cols(lax.rem(y + ny - k, ny) * CORES + core)]
        return remote(part, part, c_send.at[d, k], c_recv.at[d, k], (sp, partner))

    def copy_d(q):
        return remote(pc_send.at[q], pc_recv.at[q], d_send.at[q], d_recv.at[q], (sp, partner))

    def copy_e(q, k):
        return remote(
            ys_send.at[q, k], ys_recv.at[q, k], e_send.at[q, k], e_recv.at[q, k],
            (sp, lax.rem(y + k, ny) * CORES + core),
        )

    def copy_f(d):
        return remote(res.at[d], ret.at[d], f_send.at[d], f_recv.at[d], (lax.rem(sp + n - d, n), t))

    lane = lax.broadcasted_iota(jnp.int32, (tok, LANES), 1)
    routes = [routes_ref[:, k : k + 1] for k in range(TOPK)]
    onehot = [jnp.where(route == lane, 1.0, 0.0) for route in routes]
    below = lax.broadcasted_iota(jnp.int32, (tok, tok), 1) < lax.broadcasted_iota(jnp.int32, (tok, tok), 0)
    earlier = dot(jnp.where(below, 1.0, 0.0).astype(BF16), sum(onehot).astype(BF16))
    keys = [
        routes[k] * cap + jnp.sum(earlier * onehot[k], axis=1, keepdims=True).astype(jnp.int32)
        for k in range(TOPK)
    ]
    slot = lax.broadcasted_iota(jnp.int32, (tok, cap), 1)

    def rows_for(expert):
        wanted = slot + expert * cap
        chosen = jnp.where(keys[0] == wanted, 1.0, 0.0)
        for key in keys[1:]:
            chosen = chosen + jnp.where(key == wanted, 1.0, 0.0)
        return lax.dot_general(
            chosen.astype(BF16), normed_ref[...], (((0,), (0,)), ((), ())), preferred_element_type=F32
        ).astype(BF16)

    for d in range(1, n):
        sent[d] = rows_for(lax.rem(sp + d, n))
        if d == 1:
            pl.semaphore_wait(barrier, len(peers))
        copy_a(d).start()
    x[0, :, cols(t)] = rows_for(sp)

    def forward_a(q):
        for d in range(q * group, (q + 1) * group):
            if d:
                copy_a(d).wait_recv()
            for k in range(1, ny):
                copy_b(d, k).start()
            copy_c(d, 0).start()

    def finish(q):
        total = mine[q]
        for k in range(1, ny):
            copy_e(q, k).wait_recv()
            total = total + ys_recv[q, k].astype(F32)
        total = total.astype(BF16)
        for i in range(group):
            d = q * group + i
            block = total[i * cap : (i + 1) * cap]
            if d:
                res[d] = block
                copy_f(d).start()
            else:
                ret[0] = block

    forward_a(0)
    for q in range(chunks):
        members = range(q * group, (q + 1) * group)
        if q + 1 < chunks:
            forward_a(q + 1)
        for d in members:
            for k in range(1, ny):
                copy_b(d, k).wait_recv()
                copy_c(d, k).start()
        for d in members:
            for k in range(ny):
                copy_c(d, k).wait_recv()
        if q == 0:
            loads[0].wait()
            loads[1].wait()

        step = min(width, 256)

        @pl.loop(0, width // step)
        def _(i):
            part = pl.ds(pl.multiple_of(i * step, LANES), step)
            chosen = x[q * group : (q + 1) * group].reshape(rows, x.shape[2])
            gate = jnp.minimum(dot(chosen, wg[:, part]), GATE_LIMIT)
            up = jnp.clip(dot(chosen, wu[:, part]), -GATE_LIMIT, GATE_LIMIT)
            hidden[:, part] = ((up + 1.0) * gate * jax.nn.sigmoid(GATE_ALPHA * gate)).astype(BF16)

        if q == 0:
            loads[2].wait()
        for k in range(ny):
            block = lax.rem(y + k, ny) * CORES + (1 - core)
            pc_send[q, :, k * feat : (k + 1) * feat] = dot(hidden[...], wd[:, cols(block)]).astype(BF16)
        copy_d(q).start()
        for k in range(ny):
            block = lax.rem(y + k, ny) * CORES + core
            own[:, k * feat : (k + 1) * feat] = dot(hidden[...], wd[:, cols(block)])
        if q:
            finish(q - 1)
        copy_d(q).wait_recv()
        for k in range(1, ny):
            part = slice(k * feat, (k + 1) * feat)
            ys_send[q, k] = (own[:, part] + pc_recv[q, :, part].astype(F32)).astype(BF16)
            copy_e(q, k).start()
        mine[q] = own[:, :feat] + pc_recv[q, :, :feat].astype(F32)
    finish(chunks - 1)

    heads = [weight_ref[:, k : k + 1].astype(BF16).astype(F32) for k in range(TOPK)]
    rests = [weight_ref[:, k : k + 1] - heads[k] for k in range(TOPK)]
    acc[...] = stream_ref[...].astype(F32)
    for d in range(n):
        if d:
            copy_f(d).wait_recv()
        wanted = slot + lax.rem(sp + d, n) * cap
        high = sum(jnp.where(keys[k] == wanted, heads[k], 0.0) for k in range(TOPK))
        low = sum(jnp.where(keys[k] == wanted, rests[k], 0.0) for k in range(TOPK))
        block = ret[d]
        acc[...] += dot(high.astype(BF16), block) + dot(low.astype(BF16), block)
    out_ref[...] = acc[...].astype(BF16)

    for d in range(n):
        if d:
            copy_a(d).wait_send()
            copy_f(d).wait_send()
        for k in range(ny):
            if k:
                copy_b(d, k).wait_send()
            copy_c(d, k).wait_send()
    for q in range(chunks):
        copy_d(q).wait_send()
        for k in range(1, ny):
            copy_e(q, k).wait_send()


def moe(stream, normed, routes, route_weight, expert_gate, expert_up, expert_down):
    n, tp = lax.axis_size("sp"), lax.axis_size("tp")
    tok, feat = normed.shape
    model, width = expert_gate.shape[1:]
    cap = 2 * tok * TOPK // n
    ny = tp // CORES
    group = min(n, max(1, CHUNK_ROWS // cap))
    chunks = n // group
    rows = group * cap
    sems = pltpu.SemaphoreType.DMA
    vmem = pl.BlockSpec(memory_space=pltpu.VMEM)
    hbm = pl.BlockSpec(memory_space=pl.ANY)
    return pl.pallas_call(
        functools.partial(moe_kernel, n, tp, cap),
        out_shape=jax.ShapeDtypeStruct((tok, feat), BF16),
        in_specs=[vmem] * 4 + [hbm] * 3,
        out_specs=vmem,
        scratch_shapes=[
            pltpu.VMEM((n, cap, model), BF16),
            pltpu.VMEM((n, cap, feat), BF16),
            pltpu.VMEM((model, width), BF16),
            pltpu.VMEM((model, width), BF16),
            pltpu.VMEM((width, model), BF16),
            pltpu.VMEM((rows, width), BF16),
            pltpu.VMEM((rows, ny * feat), F32),
            pltpu.VMEM((chunks, rows, feat), F32),
            pltpu.VMEM((chunks, rows, ny * feat), BF16),
            pltpu.VMEM((chunks, rows, ny * feat), BF16),
            pltpu.VMEM((chunks, ny, rows, feat), BF16),
            pltpu.VMEM((chunks, ny, rows, feat), BF16),
            pltpu.VMEM((n, cap, feat), BF16),
            pltpu.VMEM((n, cap, feat), BF16),
            pltpu.VMEM((tok, feat), F32),
            sems((3,)),
            sems((n,)), sems((n,)),
            sems((n, ny)), sems((n, ny)),
            sems((n, ny)), sems((n, ny)),
            sems((chunks,)), sems((chunks,)),
            sems((chunks, ny)), sems((chunks, ny)),
            sems((n,)), sems((n,)),
        ],
        compiler_params=pltpu.CompilerParams(
            collective_id=0, has_side_effects=True, vmem_limit_bytes=56 * 1024 * 1024
        ),
    )(stream, normed, routes, route_weight, expert_gate, expert_up, expert_down)


def on_device(
    pool_input, pool_weight, pool_gain, out_weight, resid, norm_gain,
    routes, route_weight, expert_gate, expert_up, expert_down,
):
    tok_rows, channels = pool_input.shape
    groups = pool_weight.shape[0]
    model = expert_gate.shape[1]
    tail_rows = pool_input[tok_rows - (REACH - 1) :]
    before = from_behind(tail_rows, "sp", 1)
    extended = jnp.concatenate([before, pool_input], axis=0).astype(F32)
    first_group = lax.axis_index("tp") * groups
    width_of = 2 ** (1 + (first_group + jnp.arange(channels, dtype=jnp.int32) // GSIZE) % 4)
    position = lax.axis_index("sp") * tok_rows + jnp.arange(tok_rows, dtype=jnp.int32)
    pooled = window_pool(extended, width_of, position, tok_rows)
    grouped = jnp.einsum(
        "tgc,gcd->tgd",
        pooled.reshape(tok_rows, groups, GSIZE),
        pool_weight,
        preferred_element_type=F32,
    )
    mixed_out = (
        (grouped * pool_gain.astype(F32).reshape(groups, GSIZE)).astype(BF16).reshape(tok_rows, channels)
    )
    projected = dot(lax.all_gather(mixed_out, "tp", axis=1, tiled=True), out_weight)
    stored = lax.optimization_barrier((resid.astype(F32) + projected).astype(BF16))
    stream = stored.astype(F32)
    squares = lax.psum(jnp.sum(stream * stream, axis=1), "tp")
    scale_row = lax.rsqrt(squares / model + NORM_EPS)
    normed = (stream * scale_row[:, None] * norm_gain.astype(F32)).astype(BF16)
    return moe(stored, normed, routes, route_weight, expert_gate, expert_up, expert_down)


def solution(mesh):
    in_specs = (
        P("sp", "tp"),
        P("tp", None, None),
        P("tp"),
        P(None, "tp"),
        P("sp", "tp"),
        P("tp"),
        P("sp", None),
        P("sp", None),
        P("sp", None, "tp"),
        P("sp", None, "tp"),
        P("sp", "tp", None),
    )
    return jax.shard_map(on_device, mesh=mesh, in_specs=in_specs, out_specs=P("sp", "tp"), check_vma=False)
```

time: 211 us -> 109 us (0.52)
  waiting for transfers between devices: 103 us -> 0.01 us
  Pallas kernels: 0 us -> 79.3 us
  blocking collectives: 41.7 us -> 12.5 us
  matrix products: 21.9 us -> 2.54 us
  between operations: 13.7 us -> 0.07 us
  local copies, waits for them, and re-layouts: 11.7 us -> 5.44 us
  starting transfers between devices: 10.4 us -> 4.86 us
  other arithmetic: 7.86 us -> 3.38 us
    pallas_call x0 -> x1, Pallas kernels: none -> 79.3 us  [moe(): pl.pallas_call(functools.partial(moe_kernel, n, tp, cap), out_shape=jax.S...]
    reduce_scatter x1 -> x0, waiting for transfers between devices: 44.6 us -> none  [on_device(): lax.psum_scatter(lax.dot_general(down_piece, hidden, (((0,), (1,)), ((),...]
    all_gather x1 -> x0, waiting for transfers between devices: 33.6 us -> none  [on_device(): lax.all_gather(lax.all_to_all(sent_rows, 'sp', split_axis=0, concat_axis=...]
    all_to_all x1 -> x0, blocking collectives: 29.1 us -> none  [on_device(): lax.all_to_all(sent_rows, 'sp', split_axis=0, concat_axis=0, tiled=True)]
    all_to_all x1 -> x0, waiting for transfers between devices: 25.1 us -> none  [on_device(): lax.all_to_all(result, 'sp', split_axis=1, concat_axis=1, tiled=True)]
    dot_general x4 -> x1, matrix products: 20.6 us -> 1.2 us  [dot(): return jnp.dot(a, b, preferred_element_type=F32)]
    gather x3 -> x0, local copies, waits for them, and re-layouts: 6.13 us -> none  [the longest x1 3.97 us: on_device(): jnp.take(normed_part, slot_token, axis=0, mode='fill', fill_value=0)]
    all_to_all x1 -> x0, starting transfers between devices: 5.52 us -> none  [on_device(): lax.all_to_all(result, 'sp', split_axis=1, concat_axis=1, tiled=True)]
  transfers between devices with their start and end apart: 4 -> 1, of which waited for: 3 -> 0; matrix products, arithmetic and copies ran while one was open for 4% -> 4% of each run, Pallas kernels for 0% -> 0%
where the time goes in v1:
time: 109 us; the launch traced here: 108 us
  Pallas kernels  79.3 us (73%)
  blocking collectives  12.5 us (11%)
  local copies, waits for them, and re-layouts  5.44 us (5%)
  starting transfers between devices  4.86 us (4%)
  other arithmetic  3.38 us (3%)
  matrix products  2.54 us (2%)
    pallas_call x1, Pallas kernels, moe(): pl.pallas_call(functools.partial(moe_kernel, n, tp, cap), out_shape=jax.S...  79.3 us
    psum x1, blocking collectives, on_device(): squares = lax.psum(jnp.sum(stream * stream, axis=1), 'tp')  7.12 us
    all_gather x1, blocking collectives, on_device(): lax.all_gather(mixed_out, 'tp', axis=1, tiled=True)  5.41 us
    ppermute x1, starting transfers between devices, from_behind(): lax.ppermute(value, axis, [(source, source + steps) for source in range(f...  4.86 us
    unnamed x7, local copies, waits for them, and re-layouts  4.61 us
  transfers between devices with their start and end apart: 1, of which 0 were waited for; matrix products, arithmetic and copies ran while one was open for 4% of the time, Pallas kernels for 0%

profile of v1, /device:TPU:0, one launch (start us, length us, event | category | flops | bytes accessed | tf_op | source)
XLA Modules:
  0.0 108.1 jit_solution(10146164322943649126)
XLA Ops:
  0.0 0.0 copy-start
  0.0 0.8 slice.52
  0.8 4.9 %collective-permute-start = (bf16[15,64]{0,1:T(8,128)(2,1)S(1)}, bf16[15,64]{0,1:T(8,128)(2,1)S(1)}, u32[]{:S(2)}, u32[]{:S(2)}) collective-permute-start(bf16[15,64]{0,1:T(8,128)(2,1)S(1)} %slice.52), channel_id=1, source_target_pairs={{0,4},{4,8},{8,12},{12,16},{16,20},{20,24},{24,28},{1,5},{5,9},{9,... | collective-permute-start | bytes 5768 | tf_op jit(solution)/shard_map/ppermute | solution.py:29
  6.0 0.7 convert_element_type.37
  6.6 0.7 convert_element_type.42
  7.3 1.5 %copy.12.routes_ref = s32[256,2]{1,0:T(8,128)} copy(s32[256,2]{0,1:T(2,128)} %param.17) | data formatting | bytes 4096 | tf_op args[6]
  8.8 1.5 %copy.13.weight_ref = f32[256,2]{1,0:T(8,128)} copy(f32[256,2]{0,1:T(2,128)} %param.18) | data formatting | bytes 4096 | tf_op args[7]
  10.2 0.0 collective-permute-done
  10.2 0.8 maximum_convert_fusion
  11.1 1.3 %fusion.3 = bf16[256,1,64]{0,2,1:T(8,128)(2,1)S(1)} fusion(f32[64]{0:T(128)S(1)} %convert_element_type.37, f32[271,64]{0,1:T(8,128)S(1)} %maximum_convert_fusion, s32[64]{0:T(128)S(1)} %compare_select_fusion.7, s32[256]{0:T(256)S(1)} %add_add_fusion, pred[64]{0:T(512)(128)(4,1)S(1)} %get-tuple-element.5, pred[64]{0:T(512)(128)(4,1)S(1)} %get-tuple-element.6, ...), kind=kOutput, calls=%fused_computation.5 | convolution fusion | flops 2719744 | bytes 1099776 | tf_op jit(solution)/shard_map/tgc,gcd->tgd/dot_general | solution.py:294
  12.4 5.4 %all-gather = bf16[256,1,256]{0,2,1:T(8,128)(2,1)S(1)} all-gather(bf16[256,1,64]{0,2,1:T(8,128)(2,1)S(1)} %fusion.3), channel_id=2, replica_groups=mesh['sp'=8,'tp'=4] {'tp'}, dimensions={2}, use_global_device_ids=true | all-gather | bytes 163840 | tf_op jit(solution)/shard_map/all_gather | solution.py:303
  17.8 0.0 copy-done
  17.8 1.2 %fusion.stream_ref = bf16[256,512]{1,0:T(8,128)(2,1)S(1)} fusion(bf16[256,512]{1,0:T(8,128)(2,1)S(1)} %copy-done, bf16[256,512]{1,0:T(8,128)(2,1)} %param.15, bf16[256,1,256]{0,2,1:T(8,128)(2,1)S(1)} %all-gather), kind=kOutput, calls=%fused_computation.1 | convolution fusion | flops 67502080 | bytes 917504 | tf_op jit(solution)/shard_map/dot_general | solution.py:44
  19.0 0.0 copy-start.1
  19.0 0.1 fusion.4
  19.2 7.1 %psum.7 = f32[256]{0:T(256)S(1)} all-reduce(f32[256]{0:T(256)S(1)} %fusion.4), channel_id=1, replica_groups=mesh['sp'=8,'tp'=4] {'tp'}, use_global_device_ids=true, to_apply=%region_1.2 | all-reduce | flops 256 | bytes 2048 | tf_op jit(solution)/shard_map/psum | solution.py:306
  26.3 0.8 fusion.6.normed_ref
  27.1 0.0 copy-done.1
  27.1 79.3 %shard_map.109 = bf16[256,512]{1,0:T(8,128)(2,1)} custom-call(bf16[256,512]{1,0:T(8,128)(2,1)} %copy-done.1, bf16[256,512]{1,0:T(8,128)(2,1)} %fusion.6.normed_ref, s32[256,2]{1,0:T(8,128)} %copy.12.routes_ref, f32[256,2]{1,0:T(8,128)} %copy.13.weight_ref, bf16[1,2048,1024]{2,1,0:T(8,128)(2,1)} %gate_hbm.1, bf16[1,2048,1024]{2,1,0:T(8,128)(2,1)} %up_hbm.1, ...), custom_call_target="tpu_custom_call" | custom-call | tf_op jit(solution)/shard_map/pallas_call | solution.py:245
  106.5 1.7 %copy.15 = bf16[256,512]{1,0:T(8,128)(2,1)} copy(bf16[256,512]{1,0:T(8,128)(2,1)} %shard_map.109) | data formatting | bytes 524288
  (11 shorter events, 0.2 us)
Async XLA Ops:
  0.0 17.8 %copy-start = (bf16[256,512]{1,0:T(8,128)(2,1)S(1)}, bf16[256,512]{1,0:T(8,128)(2,1)}, u32[]{:S(2)}) copy-start(bf16[256,512]{1,0:T(8,128)(2,1)} %param.14) | copy-start | bytes 786436
  0.8 9.4 %collective-permute-start = (bf16[15,64]{0,1:T(8,128)(2,1)S(1)}, bf16[15,64]{0,1:T(8,128)(2,1)S(1)}, u32[]{:S(2)}, u32[]{:S(2)}) collective-permute-start(bf16[15,64]{0,1:T(8,128)(2,1)S(1)} %slice.52), channel_id=1, source_target_pairs={{0,4},{4,8},{8,12},{12,16},{16,20},{20,24},{24,28},{1,5},{5,9},{9,... | collective-permute-start | bytes 5768 | tf_op jit(solution)/shard_map/ppermute | solution.py:29
  19.0 8.1 %copy-start.1 = (bf16[256,512]{1,0:T(8,128)(2,1)}, bf16[256,512]{1,0:T(8,128)(2,1)S(1)}, u32[]{:S(2)}) copy-start(bf16[256,512]{1,0:T(8,128)(2,1)S(1)} %fusion.stream_ref) | copy-start | bytes 786436

commit v2 on v1

--- a/solution.py
+++ b/solution.py
@@ -23,36 +23,21 @@
 MESH = pl.DeviceIdType.MESH
 
 
-def from_behind(value, axis, steps):
-    count = lax.axis_size(axis)
-    first, last = (max(0, -steps), min(count, count - steps))
-    return lax.ppermute(value, axis, [(source, source + steps) for source in range(first, last)])
-
-
-def window_pool(extended, width_of, position, tok_count):
-    summed = jnp.zeros((tok_count, extended.shape[1]), F32)
-    for offset in range(REACH):
-        first_row = REACH - 1 - offset
-        shifted = extended[first_row : first_row + tok_count]
-        summed = summed + jnp.where(offset < width_of[None, :], shifted, 0.0)
-    counted = jnp.minimum(position[:, None] + 1, width_of[None, :]).astype(F32)
-    current = extended[REACH - 1 :]
-    return (summed / counted - current).astype(BF16)
-
-
 def dot(a, b):
     return jnp.dot(a, b, preferred_element_type=F32)
 
 
-def moe_kernel(
+def layer_kernel(
     n, tp, cap,
-    stream_ref, normed_ref, routes_ref, weight_ref, gate_hbm, up_hbm, down_hbm,
+    pool_ref, mix_ref, gain_ref, proj_ref, resid_ref, norm_ref, routes_ref, weight_ref, gate_hbm, up_hbm, down_hbm,
     out_ref,
+    tail, halo, packed, squares, stream_ref, normed_ref,
     x, sent, wg, wu, wd, hidden, own, mine, pc_send, pc_recv, ys_send, ys_recv, res, ret, acc,
-    w_sem, a_send, a_recv, b_send, b_recv, c_send, c_recv, d_send, d_recv, e_send, e_recv, f_send, f_recv,
+    w_sem, h_send, h_recv, m_send, m_recv, s_send, s_recv, a_send, a_recv, b_send, b_recv, c_send, c_recv, d_send, d_recv, e_send, e_recv, f_send, f_recv,
 ):
     ny = tp // CORES
-    tok, feat = normed_ref.shape
+    tok, feat = resid_ref.shape
+    channels = pool_ref.shape[1]
     width = wg.shape[1]
     group = x.shape[0] // ys_send.shape[0]
     chunks = n // group
@@ -72,8 +57,7 @@
 
     barrier = pltpu.get_barrier_semaphore()
     peers = [(lax.rem(sp + d, n), t) for d in range(1, n)]
-    peers += [(sp, lax.rem(y + k, ny) * CORES + core) for k in range(1, ny)]
-    peers += [(sp, partner)]
+    peers += [(sp, lax.rem(t + k, tp)) for k in range(1, tp)]
     for peer in peers:
         pl.semaphore_signal(barrier, inc=1, device_id=peer, device_id_type=MESH)
 
@@ -108,19 +92,82 @@
     def copy_f(d):
         return remote(res.at[d], ret.at[d], f_send.at[d], f_recv.at[d], (lax.rem(sp + n - d, n), t))
 
-    lane = lax.broadcasted_iota(jnp.int32, (tok, LANES), 1)
-    routes = [routes_ref[:, k : k + 1] for k in range(TOPK)]
+    tail_copy = remote(tail, halo, h_send.at[0], h_recv.at[0], (lax.rem(sp + 1, n), t))
+
+    def copy_m(k):
+        return remote(packed.at[0], packed.at[k], m_send.at[k], m_recv.at[k], (sp, lax.rem(t + k, tp)))
+
+    def copy_s(k):
+        return remote(squares.at[0], squares.at[k], s_send.at[k], s_recv.at[k], (sp, lax.rem(t + k, tp)))
+
+    tail[...] = jnp.zeros_like(tail)
+    tail[:, :channels] = pool_ref[tok - REACH :, :].astype(F32)
+    pl.semaphore_wait(barrier, len(peers))
+    tail_copy.start()
+
+    listed = jnp.concatenate(
+        [routes_ref[...].astype(F32), weight_ref[...], jnp.zeros((8 - 2 * TOPK, tok), F32)], axis=0
+    ).T
+    routes = [listed[:, k : k + 1] for k in range(TOPK)]
+    weights = [listed[:, TOPK + k : TOPK + k + 1] for k in range(TOPK)]
+    lane = lax.broadcasted_iota(jnp.int32, (tok, LANES), 1).astype(F32)
     onehot = [jnp.where(route == lane, 1.0, 0.0) for route in routes]
     below = lax.broadcasted_iota(jnp.int32, (tok, tok), 1) < lax.broadcasted_iota(jnp.int32, (tok, tok), 0)
     earlier = dot(jnp.where(below, 1.0, 0.0).astype(BF16), sum(onehot).astype(BF16))
     keys = [
-        routes[k] * cap + jnp.sum(earlier * onehot[k], axis=1, keepdims=True).astype(jnp.int32)
-        for k in range(TOPK)
+        routes[k] * float(cap) + jnp.sum(earlier * onehot[k], axis=1, keepdims=True) for k in range(TOPK)
     ]
     slot = lax.broadcasted_iota(jnp.int32, (tok, cap), 1)
 
+    tail_copy.wait_recv()
+    before = jnp.where(sp == 0, 0.0, halo[:, :channels])
+    current = pool_ref[...].astype(F32)
+    summed = jnp.concatenate([before, current], axis=0)
+    groups = channels // GSIZE
+    group_of = t * groups + lax.broadcasted_iota(jnp.int32, (1, channels), 1) // GSIZE
+    level = lax.rem(group_of, 4)
+    window, span = jnp.zeros((tok, channels), F32), jnp.zeros((1, channels), F32)
+    for power in range(4):
+        summed = summed + pltpu.roll(summed, 1 << power, 0)
+        window = jnp.where(level == power, summed[REACH:], window)
+        span = jnp.where(level == power, float(2 << power), span)
+    place = (sp * tok + 1 + lax.broadcasted_iota(jnp.int32, (tok, channels), 0)).astype(F32)
+    pooled = (window / jnp.minimum(place, span) - current).astype(BF16)
+    mixed = jnp.concatenate(
+        [dot(pooled[:, g * GSIZE : (g + 1) * GSIZE], mix_ref[g]) for g in range(groups)], axis=1
+    )
+    mixed = (mixed * gain_ref[...].astype(F32)).astype(BF16)
+    folds = max(1, LANES // channels)
+    short = tok // folds
+    packed[0] = jnp.concatenate([mixed[i * short : (i + 1) * short] for i in range(folds)], axis=1)
+    for k in range(1, tp):
+        copy_m(k).start()
+
+    def projected(k):
+        block = packed[k]
+        part = jnp.concatenate([block[:, i * channels : (i + 1) * channels] for i in range(folds)], axis=0)
+        first = lax.rem(t + tp - k, tp) * channels
+        return dot(part, proj_ref[pl.ds(pl.multiple_of(first, GSIZE), channels), :])
+
+    acc[...] = resid_ref[...].astype(F32) + projected(0)
+    for k in range(1, tp):
+        copy_m(k).wait_recv()
+        acc[...] += projected(k)
+    stream_ref[...] = acc[...].astype(BF16)
+    stream = stream_ref[...].astype(F32)
+    power = jnp.sum(stream * stream, axis=1, keepdims=True)
+    squares[0] = jnp.broadcast_to(power, (tok, LANES)).T[:8]
+    for k in range(1, tp):
+        copy_s(k).start()
+    total = squares[0]
+    for k in range(1, tp):
+        copy_s(k).wait_recv()
+        total = total + squares[k]
+    scale = lax.rsqrt(total.T[:, :1] / x.shape[2] + NORM_EPS)
+    normed_ref[...] = (stream_ref[...].astype(F32) * scale * norm_ref[...].astype(F32)).astype(BF16)
+
     def rows_for(expert):
-        wanted = slot + expert * cap
+        wanted = (slot + expert * cap).astype(F32)
         chosen = jnp.where(keys[0] == wanted, 1.0, 0.0)
         for key in keys[1:]:
             chosen = chosen + jnp.where(key == wanted, 1.0, 0.0)
@@ -130,8 +177,6 @@
 
     for d in range(1, n):
         sent[d] = rows_for(lax.rem(sp + d, n))
-        if d == 1:
-            pl.semaphore_wait(barrier, len(peers))
         copy_a(d).start()
     x[0, :, cols(t)] = rows_for(sp)
 
@@ -203,19 +248,23 @@
         mine[q] = own[:, :feat] + pc_recv[q, :, :feat].astype(F32)
     finish(chunks - 1)
 
-    heads = [weight_ref[:, k : k + 1].astype(BF16).astype(F32) for k in range(TOPK)]
-    rests = [weight_ref[:, k : k + 1] - heads[k] for k in range(TOPK)]
+    heads = [weight.astype(BF16).astype(F32) for weight in weights]
+    rests = [weights[k] - heads[k] for k in range(TOPK)]
     acc[...] = stream_ref[...].astype(F32)
     for d in range(n):
         if d:
             copy_f(d).wait_recv()
-        wanted = slot + lax.rem(sp + d, n) * cap
+        wanted = (slot + lax.rem(sp + d, n) * cap).astype(F32)
         high = sum(jnp.where(keys[k] == wanted, heads[k], 0.0) for k in range(TOPK))
         low = sum(jnp.where(keys[k] == wanted, rests[k], 0.0) for k in range(TOPK))
         block = ret[d]
         acc[...] += dot(high.astype(BF16), block) + dot(low.astype(BF16), block)
     out_ref[...] = acc[...].astype(BF16)
 
+    tail_copy.wait_send()
+    for k in range(1, tp):
+        copy_m(k).wait_send()
+        copy_s(k).wait_send()
     for d in range(n):
         if d:
             copy_a(d).wait_send()
@@ -230,9 +279,14 @@
             copy_e(q, k).wait_send()
 
 
-def moe(stream, normed, routes, route_weight, expert_gate, expert_up, expert_down):
+def on_device(
+    pool_input, pool_weight, pool_gain, out_weight, resid, norm_gain,
+    routes, route_weight, expert_gate, expert_up, expert_down,
+):
     n, tp = lax.axis_size("sp"), lax.axis_size("tp")
-    tok, feat = normed.shape
+    tok, feat = resid.shape
+    channels = pool_input.shape[1]
+    folds = max(1, LANES // channels)
     model, width = expert_gate.shape[1:]
     cap = 2 * tok * TOPK // n
     ny = tp // CORES
@@ -243,11 +297,17 @@
     vmem = pl.BlockSpec(memory_space=pltpu.VMEM)
     hbm = pl.BlockSpec(memory_space=pl.ANY)
     return pl.pallas_call(
-        functools.partial(moe_kernel, n, tp, cap),
+        functools.partial(layer_kernel, n, tp, cap),
         out_shape=jax.ShapeDtypeStruct((tok, feat), BF16),
-        in_specs=[vmem] * 4 + [hbm] * 3,
+        in_specs=[vmem] * 8 + [hbm] * 3,
         out_specs=vmem,
         scratch_shapes=[
+            pltpu.VMEM((REACH, max(LANES, channels)), F32),
+            pltpu.VMEM((REACH, max(LANES, channels)), F32),
+            pltpu.VMEM((tp, tok // folds, folds * channels), BF16),
+            pltpu.VMEM((tp, 8, tok), F32),
+            pltpu.VMEM((tok, feat), BF16),
+            pltpu.VMEM((tok, feat), BF16),
             pltpu.VMEM((n, cap, model), BF16),
             pltpu.VMEM((n, cap, feat), BF16),
             pltpu.VMEM((model, width), BF16),
@@ -264,6 +324,9 @@
             pltpu.VMEM((n, cap, feat), BF16),
             pltpu.VMEM((tok, feat), F32),
             sems((3,)),
+            sems((1,)), sems((1,)),
+            sems((tp,)), sems((tp,)),
+            sems((tp,)), sems((tp,)),
             sems((n,)), sems((n,)),
             sems((n, ny)), sems((n, ny)),
             sems((n, ny)), sems((n, ny)),
@@ -274,39 +337,10 @@
         compiler_params=pltpu.CompilerParams(
             collective_id=0, has_side_effects=True, vmem_limit_bytes=56 * 1024 * 1024
         ),
-    )(stream, normed, routes, route_weight, expert_gate, expert_up, expert_down)
-
-
-def on_device(
-    pool_input, pool_weight, pool_gain, out_weight, resid, norm_gain,
-    routes, route_weight, expert_gate, expert_up, expert_down,
-):
-    tok_rows, channels = pool_input.shape
-    groups = pool_weight.shape[0]
-    model = expert_gate.shape[1]
-    tail_rows = pool_input[tok_rows - (REACH - 1) :]
-    before = from_behind(tail_rows, "sp", 1)
-    extended = jnp.concatenate([before, pool_input], axis=0).astype(F32)
-    first_group = lax.axis_index("tp") * groups
-    width_of = 2 ** (1 + (first_group + jnp.arange(channels, dtype=jnp.int32) // GSIZE) % 4)
-    position = lax.axis_index("sp") * tok_rows + jnp.arange(tok_rows, dtype=jnp.int32)
-    pooled = window_pool(extended, width_of, position, tok_rows)
-    grouped = jnp.einsum(
-        "tgc,gcd->tgd",
-        pooled.reshape(tok_rows, groups, GSIZE),
-        pool_weight,
-        preferred_element_type=F32,
+    )(
+        pool_input, pool_weight, pool_gain.reshape(1, -1), out_weight, resid, norm_gain.reshape(1, -1),
+        routes.T, route_weight.T, expert_gate, expert_up, expert_down,
     )
-    mixed_out = (
-        (grouped * pool_gain.astype(F32).reshape(groups, GSIZE)).astype(BF16).reshape(tok_rows, channels)
-    )
-    projected = dot(lax.all_gather(mixed_out, "tp", axis=1, tiled=True), out_weight)
-    stored = lax.optimization_barrier((resid.astype(F32) + projected).astype(BF16))
-    stream = stored.astype(F32)
-    squares = lax.psum(jnp.sum(stream * stream, axis=1), "tp")
-    scale_row = lax.rsqrt(squares / model + NORM_EPS)
-    normed = (stream * scale_row[:, None] * norm_gain.astype(F32)).astype(BF16)
-    return moe(stored, normed, routes, route_weight, expert_gate, expert_up, expert_down)
 
 
 def solution(mesh):

time: 109 us -> 96.7 us (0.89)
  Pallas kernels: 79.3 us -> 92 us
  blocking collectives: 12.5 us -> 0 us
  starting transfers between devices: 4.86 us -> 0 us
  other arithmetic: 3.38 us -> 0 us
  matrix products: 2.54 us -> 0 us
    pallas_call x1, Pallas kernels: 79.3 us -> 92 us  [on_device(): pl.pallas_call(functools.partial(layer_kernel, n, tp, cap), out_shape=jax...]
    psum x1 -> x0, blocking collectives: 7.12 us -> none  [on_device(): squares = lax.psum(jnp.sum(stream * stream, axis=1), 'tp')]
    all_gather x1 -> x0, blocking collectives: 5.41 us -> none  [on_device(): lax.all_gather(mixed_out, 'tp', axis=1, tiled=True)]
    ppermute x1 -> x0, starting transfers between devices: 4.86 us -> none  [from_behind(): lax.ppermute(value, axis, [(source, source + steps) for source in range(f...]
    convert_element_type x4 -> x0, other arithmetic: 3.02 us -> none  [the longest x2 1.52 us: on_device(): normed = (stream * scale_row[:, None] * norm_gain.astype(F32)).astype(BF16)]
    dot_general x2 -> x0, matrix products: 2.54 us -> none  [the longest x1 1.34 us: on_device(): jnp.einsum('tgc,gcd->tgd', pooled.reshape(tok_rows, groups, GSIZE), pool_...]
    unnamed x7 -> x2, local copies, waits for them, and re-layouts: 4.61 us -> 3.16 us
    reshape x0 -> x1, local copies, waits for them, and re-layouts: none -> 1.25 us  [on_device(): norm_gain.reshape(1, -1)]
  transfers between devices with their start and end apart: 1 -> 0, of which waited for: 0 -> 0; matrix products, arithmetic and copies ran while one was open for 4% -> 0% of each run, Pallas kernels for 0% -> 0%
where the time goes in v2:
time: 96.7 us; the launch traced here: 96.5 us
  Pallas kernels  92 us (95%)
  local copies, waits for them, and re-layouts  4.41 us (5%)
    pallas_call x1, Pallas kernels, on_device(): pl.pallas_call(functools.partial(layer_kernel, n, tp, cap), out_shape=jax...  92 us
    unnamed x2, local copies, waits for them, and re-layouts  3.16 us

profile of v2, /device:TPU:0, one launch (start us, length us, event | category | flops | bytes accessed | tf_op | source)
XLA Modules:
  0.0 96.5 jit_solution(12575461494604412282)
XLA Ops:
  0.0 1.3 %reshape.7.norm_ref = bf16[1,512]{1,0:T(2,128)(2,1)} reshape(bf16[512]{0:T(512)(128)(2,1)} %param.16) | data formatting | bytes 2048 | tf_op jit(solution)/shard_map/reshape | solution.py:341
  1.3 1.5 %copy.12.pool_ref = bf16[256,64]{1,0:T(8,128)(2,1)} copy(bf16[256,64]{0,1:T(8,128)(2,1)} %param.11) | data formatting | bytes 65536 | tf_op args[0]
  2.7 92.0 %shard_map.109 = bf16[256,512]{1,0:T(8,128)(2,1)} custom-call(bf16[256,64]{1,0:T(8,128)(2,1)} %copy.12.pool_ref, bf16[1,64,64]{2,1,0:T(8,128)(2,1)} %mix_ref.1, bf16[1,64]{1,0:T(2,128)(2,1)} %bitcast.5, bf16[256,512]{1,0:T(8,128)(2,1)} %proj_ref.1, bf16[256,512]{1,0:T(8,128)(2,1)} %resid_ref.1, bf16[1,512]{1,0:T(2,128)(2,1)} %reshape.7.norm_ref, ...), custom_call_target="tpu_custom_call" | custom-call | tf_op jit(solution)/shard_map/pallas_call | solution.py:299
  94.8 1.7 %copy.14 = bf16[256,512]{1,0:T(8,128)(2,1)} copy(bf16[256,512]{1,0:T(8,128)(2,1)} %shard_map.109) | data formatting | bytes 524288
